TPU v7x, 128 devices: a whole 4x4x4 slice. The times are simulated.
128 devices in a mesh: rep: 2 (over z_hi), fs: 32 (over z_lo, y, x), tp: 2 (over core).
Axes of the slice: x: 4, y: 4, z: 4 (z_hi: 2, z_lo: 2; z = z_hi * 2 + z_lo), core: 2. Of those that a mesh axis runs over, the one named last changes fastest.
Arguments:
- tokens: bfloat16 [32768, 2048], P(('rep', 'fs'), 'tp'), may hold values from -6 to 6
- mix_gain: float32 [2048], replicated, may hold values from 0.1 to 1.9
- lru_input: float32 [2048, 2048], P('fs', 'tp'), may hold values from -0.125 to 0.125
- lru_gate: float32 [2048, 2048], P('fs', 'tp'), may hold values from -0.125 to 0.125
- lru_input_scale: float32 [2048], P('tp'), may hold values from 0.5 to 2
- lru_gate_scale: float32 [2048], P('tp'), may hold values from 0.5 to 2
- conv_weight: float32 [4, 2048], P(None, 'tp'), may hold values from -3 to 3
- recur_gate: float32 [32, 64, 64], P('tp'), may hold values from -0.75 to 0.75
- input_gate: float32 [32, 64, 64], P('tp'), may hold values from -0.75 to 0.75
- decay_rate: float32 [2048], P('tp'), may hold values from 3.5 to 9
- extra_decay: float32 [32768], P(('rep', 'fs')), may hold values from 0.0003 to 2.1
- lru_output: float32 [2048, 2048], P('tp', 'fs'), may hold values from -0.125 to 0.125
- lru_output_scale: float32 [2048], replicated, may hold values from 0.5 to 2
- ffn_gain: float32 [2048], replicated, may hold values from 0.1 to 1.9
- ffn_gate: float32 [2048, 2816], P('fs', 'tp'), may hold values from -0.125 to 0.125
- ffn_up: float32 [2048, 2816], P('fs', 'tp'), may hold values from -0.125 to 0.125
- ffn_gate_scale: float32 [2816], P('tp'), may hold values from 0.5 to 2
- ffn_up_scale: float32 [2816], P('tp'), may hold values from 0.5 to 2
- ffn_down: float32 [2816, 2048], P('tp', 'fs'), may hold values from -0.109375 to 0.109375
- ffn_down_scale: float32 [2048], replicated, may hold values from 0.5 to 2
Outputs:
- layer_out: bfloat16 [32768, 2048], P(('rep', 'fs'), 'tp')
All inputs are finite; a program needn't handle non-finite values.
Results may differ from a plain program's by a relative error of at most 0.02.
Values may be sent and summed in bfloat16 or wider, within the bound.
No kernel may reach another device: no remote copies, remote signals or barrier semaphores. Data moves between devices by JAX's collectives and lax.ppermute only.
A program may use at most 192 MiB of HBM per device.

v0:
```python
import jax
import jax.numpy as jnp
from jax import lax
from jax.sharding import Mesh
from jax.sharding import PartitionSpec as P

FS = ("fs_0", "fs_1", "fs_2")
REP_FS = ("rep", "fs_0", "fs_1", "fs_2")


EPS = 1e-06
RATE = 8.0


def sent_to_all(array, axis):
    copies = jnp.broadcast_to(array, (lax.axis_size(axis), *array.shape))
    return lax.all_to_all(copies, axis, split_axis=0, concat_axis=0, tiled=True)


def laid_out(blocks, dim):
    dims = list(blocks.shape[1:])
    dims[dim] *= blocks.shape[0]
    return jnp.moveaxis(blocks, 0, dim).reshape(dims)


def gather_directly(array, axis, dim):
    blocks = sent_to_all(array, axis)
    return laid_out(blocks, dim)


def split_up(array, dim, count):
    dims = array.shape
    blocks = array.reshape(*dims[:dim], count, dims[dim] // count, *dims[dim + 1 :])
    return jnp.moveaxis(blocks, dim, 0)


def sent_and_summed(array, axis, dim):
    count = lax.axis_size(axis)
    blocks = lax.all_to_all(split_up(array, dim, count), axis, 0, 0, tiled=True)
    return jnp.sum(blocks.astype(jnp.float32), axis=0)


def sent_together(arrays, axis, dim, along):
    both = jnp.concatenate(arrays, axis=along)
    whole, at, finished = (lax.all_gather(both, axis, axis=dim, tiled=True), 0, [])
    for a in arrays:
        finished.append(lax.slice_in_dim(whole, at, at + a.shape[along], axis=along))
        at += a.shape[along]
    return tuple(finished)


def all_blocks(array, axes, order):
    blocks = array[None]
    for k in order:
        blocks = lax.all_gather(blocks, axes[k], axis=0, tiled=True)
    carried = [lax.axis_size(axes[k]) for k in reversed(order)]
    blocks = blocks.reshape(*carried, *array.shape)
    turned = sorted(range(len(order)), key=lambda place: order[len(order) - 1 - place])
    return blocks.transpose(*turned, *range(len(order), blocks.ndim)).reshape(-1, *array.shape)


def gathered_by_axis(array, axes, order, dim):
    return laid_out(all_blocks(array, axes, order), dim)


def rms_rows(rows, gain):
    values = rows.astype(jnp.float32)
    scale = lax.rsqrt(jnp.mean(values * values, axis=-1, keepdims=True) + EPS)
    return (values * scale * gain).astype(jnp.bfloat16)


def combine(left, right):
    return (left[0] * right[0], right[0] * left[1] + right[1])


def block_gate(grouped, blocks, length):
    mapped = jnp.einsum("sni,nij->snj", grouped, blocks)
    return jax.nn.sigmoid(mapped.reshape(length, -1))


def full_rows(part):
    return gather_directly(part, "tp", 1)


def own_columns(terms):
    return sent_and_summed(terms.astype(jnp.bfloat16), "tp", 1)


def project_pair(normed, first, second):
    pair = (first.astype(jnp.bfloat16), second.astype(jnp.bfloat16))
    first_full, second_full = sent_together((pair[0], pair[1]), FS, 0, 1)
    return (
        jnp.dot(normed, first_full, preferred_element_type=jnp.float32),
        jnp.dot(normed, second_full, preferred_element_type=jnp.float32),
    )


def project_back(acts, weight):
    cast = weight.astype(jnp.bfloat16)
    whole = gathered_by_axis(cast, FS, (0, 1, 2), 1)
    return jnp.dot(acts, whole, preferred_element_type=jnp.float32)


def recurrence(branch_in, branch_gate, conv_weight, recur_gate, input_gate, decay_rate, extra):
    length = branch_in.shape[0]
    taps = conv_weight.shape[0]
    values = branch_in.astype(jnp.float32)
    padded = jnp.pad(values, ((taps - 1, 0), (0, 0)))
    conv = jnp.zeros_like(values)
    for tap in range(taps):
        conv = conv + conv_weight[tap] * padded[tap : tap + length]
    grouped = conv.reshape(length, recur_gate.shape[0], recur_gate.shape[1])
    recur = block_gate(grouped, recur_gate, length)
    ingate = block_gate(grouped, input_gate, length)
    log_rate = -RATE * jax.nn.softplus(-decay_rate) * recur - extra[:, None]
    factor = jnp.exp(log_rate)
    drive = jnp.sqrt(-jnp.expm1(2.0 * log_rate)) * (ingate * conv)
    state = lax.associative_scan(combine, (factor, drive), axis=0)[1]
    gelu_gate = jax.nn.gelu(branch_gate.astype(jnp.float32), approximate=True)
    return (state * gelu_gate).astype(jnp.bfloat16)


def local(
    tokens,
    mix_gain,
    lru_input,
    lru_gate,
    lru_input_scale,
    lru_gate_scale,
    conv_weight,
    recur_gate,
    input_gate,
    decay_rate,
    extra_decay,
    lru_output,
    lru_output_scale,
    ffn_gain,
    ffn_gate,
    ffn_up,
    ffn_gate_scale,
    ffn_up_scale,
    ffn_down,
    ffn_down_scale,
):
    columns = tokens.shape[1]
    offset = lax.axis_index("tp") * columns
    whole_rows = full_rows(tokens)
    normed = rms_rows(whole_rows, mix_gain)
    in_pre, gate_pre = project_pair(normed, lru_input, lru_gate)
    branch_in = (in_pre * lru_input_scale).astype(jnp.bfloat16)
    branch_gate = (gate_pre * lru_gate_scale).astype(jnp.bfloat16)
    gated = recurrence(
        branch_in, branch_gate, conv_weight, recur_gate, input_gate, decay_rate, extra_decay
    )
    terms = project_back(gated, lru_output)
    total = own_columns(terms)
    scale_part = lax.dynamic_slice_in_dim(lru_output_scale, offset, columns)
    mixed = (tokens.astype(jnp.float32) + total * scale_part).astype(jnp.bfloat16)
    mixed_rows = full_rows(mixed)
    normed2 = rms_rows(mixed_rows, ffn_gain)
    gate_val, up_val = project_pair(normed2, ffn_gate, ffn_up)
    hidden = (jax.nn.silu(gate_val * ffn_gate_scale) * (up_val * ffn_up_scale)).astype(jnp.bfloat16)
    summed = own_columns(project_back(hidden, ffn_down))
    down_part = lax.dynamic_slice_in_dim(ffn_down_scale, offset, columns)
    return (mixed.astype(jnp.float32) + summed * down_part).astype(jnp.bfloat16)


def solution(mesh):
    split = Mesh(
        mesh.devices.reshape(mesh.shape["rep"], 2, 4, 4, mesh.shape["tp"]),
        ("rep", "fs_0", "fs_1", "fs_2", "tp"),
    )
    in_specs = (
        P(REP_FS, "tp"),
        P(),
        P(FS, "tp"),
        P(FS, "tp"),
        P("tp"),
        P("tp"),
        P(None, "tp"),
        P("tp", None, None),
        P("tp", None, None),
        P("tp"),
        P(REP_FS),
        P("tp", FS),
        P(),
        P(),
        P(FS, "tp"),
        P(FS, "tp"),
        P("tp"),
        P("tp"),
        P("tp", FS),
        P(),
    )
    out_specs = P(REP_FS, "tp")
    return jax.shard_map(local, mesh=split, in_specs=in_specs, out_specs=out_specs, check_vma=False)
```

profile of v0, /device:TPU:1, one launch (start us, length us, event | category | flops | bytes accessed | tf_op | source)
XLA Modules:
  0.0 565.5 jit_solution(1838571929659336265)
XLA Ops:
  7.6 6.3 %all-gather = bf16[2048,64]{0,1:T(8,128)(2,1)S(1)} all-gather(bf16[1024,64]{0,1:T(8,128)(2,1)S(1)} %convert_element_type.107), channel_id=2, replica_groups=mesh['rep'=2,'fs_0'=2,'fs_1'=4,'fs_2'=4,'tp'=2] {'fs_0'}, dimensions={0}, use_global_device_ids=true | all-gather | bytes 393216 | tf_op jit(solution)/shard_map/all_gather | solution.py:55
  15.7 5.6 all-gather.1
  22.2 17.4 %all-gather.11.cloned.1.call-done = bf16[8,1024,64]{1,2,0:T(8,128)(2,1)} async-done(((bf16[2,1024,64]{1,2,0:T(8,128)(2,1)}), bf16[8,1024,64]{1,2,0:T(8,128)(2,1)}) %all-gather.11.cloned.1.call-update) | async-done | bytes 1048592 | tf_op jit(solution)/shard_map/all_gather | solution.py:55
  39.7 29.3 %all-gather.17.cloned.1.call-done = bf16[8,1408,64]{1,2,0:T(8,128)(2,1)} async-done(((bf16[2,1408,64]{1,2,0:T(8,128)(2,1)}), bf16[8,1408,64]{1,2,0:T(8,128)(2,1)}) %all-gather.17.cloned.1.call-update) | async-done | bytes 1441808 | tf_op jit(solution)/shard_map/all_gather | solution.py:55
  72.8 4.6 all-to-all-start
  82.3 36.9 %all-gather.13.cloned.1.call-done = bf16[32,1024,64]{1,2,0:T(8,128)(2,1)} async-done(((bf16[8,1024,64]{1,2,0:T(8,128)(2,1)}), bf16[32,1024,64]{1,2,0:T(8,128)(2,1)}) %all-gather.13.cloned.1.call-update) | async-done | bytes 4194320 | tf_op jit(solution)/shard_map/all_gather | solution.py:55
  119.2 4.8 copy.74
  124.0 58.3 %all-gather.19.cloned.1.call-done = bf16[32,1408,64]{1,2,0:T(8,128)(2,1)} async-done(((bf16[8,1408,64]{1,2,0:T(8,128)(2,1)}), bf16[32,1408,64]{1,2,0:T(8,128)(2,1)}) %all-gather.19.cloned.1.call-update) | async-done | bytes 5767184 | tf_op jit(solution)/shard_map/all_gather | solution.py:55
  182.3 5.8 %copy.78 = bf16[2,4,4,1408,64]{3,4,2,1,0:T(8,128)(2,1)} copy(bf16[2,4,4,1408,64]{3,4,0,1,2:T(8,128)(2,1)} %bitcast.83) | data formatting | bytes 11534336 | tf_op jit(solution)/shard_map/transpose | solution.py:59
  188.2 142.3 %all-gather.9.cloned.1.call-done = bf16[2048,2048]{1,0:T(8,128)(2,1)} async-done(((bf16[64,2048]{1,0:T(8,128)(2,1)}), bf16[2048,2048]{1,0:T(8,128)(2,1)}) %all-gather.9.cloned.1.call-update) | async-done | bytes 8388624 | tf_op jit(solution)/shard_map/all_gather | solution.py:45
  330.5 4.5 fusion.37
  346.5 8.7 %fusion.32 = (f32[512,1024]{1,0:T(8,128)}, f32[512,1024]{1,0:T(8,128)S(1)}) fusion(f32[512,1024]{1,0:T(8,128)} %copy.70, f32[512]{0:T(512)S(1)} %copy-done.32, f32[1024]{0:T(1024)S(1)} %fusion.53, f32[512,1024]{1,0:T(8,128)} %copy.72, f32[512,1024]{1,0:T(8,128)} %copy-done.2, f32[1024]{0:T(1024)S(1)} %bitcast.101, f32[1024]{0:T(1024)S(1)} %bitcast.103, ...), kind=kLoop, calls=%fused_computation.48 | loop fusion | flops 6815744 | bytes 10508288 | tf_op jit(solution)/shard_map/exp | solution.py:116
  360.8 5.4 slice.251
  366.2 5.4 slice.255
  371.6 4.1 fusion.59
  450.7 5.5 slice.250
  464.3 8.6 %pad.77 = f32[512,1024]{1,0:T(8,128)} pad(f32[256,1024]{1,0:T(8,128)} %add.211, f32[]{:T(128)} %constant.13.clone.1), padding=1_0_1x0_0_0 | pad | bytes 3145732 | tf_op jit(solution)/shard_map/pad | solution.py:118
  475.0 4.8 pad.76
  479.8 10.5 %convolution_convert_fusion = bf16[512,2048]{1,0:T(8,128)(2,1)S(1)} fusion(bf16[1024,2048]{0,1:T(8,128)(2,1)} %bitcast.84, f32[512,1024]{1,0:T(8,128)} %pad.76, f32[512,1024]{1,0:T(8,128)} %pad.77, bf16[512,2048]{0,1:T(8,128)(2,1)} %fusion.11, bf16[2048,2048]{1,0:T(8,128)(2,1)} %all-gather.9.cloned.1.call-done, f32[1024]{0:T(1024)S(1)} %copy-done.37), kind=kOutput, calls=%fused_computation.25 | convolution fusion | flops 4303355904 | bytes 16781312 | tf_op jit(solution)/shard_map/dot_general | solution.py:101
  490.5 26.0 %all_to_all.20 = bf16[2,512,1024]{2,1,0:T(8,128)(2,1)S(1)} all-to-all(bf16[2,512,1024]{2,1,0:T(8,128)(2,1)S(1)} %bitcast.80), channel_id=1, replica_groups=mesh['rep'=2,'fs_0'=2,'fs_1'=4,'fs_2'=4,'tp'=2] {'tp'}, dimensions={0} | all-to-all | bytes 4194304 | tf_op jit(solution)/shard_map/all_to_all | solution.py:39
  518.8 5.6 all_to_all.21
  527.0 8.3 %fusion.12 = f32[512,1408]{1,0:T(8,128)} fusion(bf16[512,2048]{0,1:T(8,128)(2,1)} %fusion.9, bf16[2048,2816]{1,0:T(8,128)(2,1)} %all-gather.15.cloned.1.call-done, f32[1408]{0:T(1024)S(1)} %copy-done.34), kind=kOutput, calls=%fused_computation.22 | convolution fusion | flops 2953510912 | bytes 10753536 | tf_op jit(solution)/shard_map/dot_general | solution.py:93
  535.3 14.2 %convolution_convert_fusion.1 = bf16[512,2048]{1,0:T(8,128)(2,1)} fusion(bf16[1408,2048]{0,1:T(8,128)(2,1)} %bitcast.82, bf16[512,2048]{0,1:T(8,128)(2,1)} %fusion.9, bf16[2048,2816]{1,0:T(8,128)(2,1)} %all-gather.15.cloned.1.call-done, f32[512,1408]{1,0:T(8,128)} %fusion.12, f32[1408]{0:T(1024)S(1)} %copy-done.35), kind=kOutput, calls=%fused_computation.27 | convolution fusion | flops 5911674880 | bytes 18617856 | tf_op jit(solution)/shard_map/dot_general | solution.py:101
  551.3 5.3 all_to_all.22
  (224 shorter events, 122.8 us)
Async XLA Ops:
  6.5 332.3 %copy-start = (f32[16,64,64]{2,1,0:T(8,128)S(1)}, f32[16,64,64]{2,1,0:T(8,128)}, u32[]{:S(2)}) copy-start(f32[16,64,64]{2,1,0:T(8,128)} %param.27) | copy-start | bytes 786436
  6.5 33.1 %all-gather.11.cloned.1.call-start = ((), (), s32[]{:S(2)}) async-start(), calls=%async_computation.5 | async-start | bytes 1310720 | tf_op jit(solution)/shard_map/all_gather | solution.py:55
  14.6 54.3 %all-gather.17.cloned.1.call-start = ((), (), s32[]{:S(2)}) async-start(), calls=%async_computation.8 | async-start | bytes 1802240 | tf_op jit(solution)/shard_map/all_gather | solution.py:55
  15.7 53.3 %copy-start.13 = (f32[64,1024]{1,0:T(8,128)S(1)}, f32[64,1024]{1,0:T(8,128)}, u32[]{:S(2)}) copy-start(f32[64,1024]{1,0:T(8,128)} %param.22) | copy-start | bytes 786436
  21.3 47.7 %copy-start.14 = (f32[64,1024]{1,0:T(8,128)S(1)}, f32[64,1024]{1,0:T(8,128)}, u32[]{:S(2)}) copy-start(f32[64,1024]{1,0:T(8,128)} %param.23) | copy-start | bytes 786436
  22.1 47.8 %copy-start.10 = (f32[64,1408]{1,0:T(8,128)S(1)}, f32[64,1408]{1,0:T(8,128)}, u32[]{:S(2)}) copy-start(f32[64,1408]{1,0:T(8,128)} %param.34) | copy-start | bytes 1081348
  22.1 97.0 %all-gather.13.cloned.1.call-start = ((), (), s32[]{:S(2)}) async-start(), calls=%async_computation.6 | async-start | bytes 5242880 | tf_op jit(solution)/shard_map/all_gather | solution.py:55
  39.6 30.3 %copy-start.11 = (f32[64,1408]{1,0:T(8,128)S(1)}, f32[64,1408]{1,0:T(8,128)}, u32[]{:S(2)}) copy-start(f32[64,1408]{1,0:T(8,128)} %param.35) | copy-start | bytes 1081348
  39.6 142.7 %all-gather.19.cloned.1.call-start = ((), (), s32[]{:S(2)}) async-start(), calls=%async_computation.9 | async-start | bytes 7208960 | tf_op jit(solution)/shard_map/all_gather | solution.py:55
  69.0 261.5 %all-gather.9.cloned.1.call-start = ((), (), s32[]{:S(2)}) async-start(), calls=%async_computation.4 | async-start | bytes 8650752 | tf_op jit(solution)/shard_map/all_gather | solution.py:45
  69.8 457.2 %all-gather.15.cloned.1.call-start = ((), (), s32[]{:S(2)}) async-start(), calls=%async_computation.7 | async-start | bytes 11894784 | tf_op jit(solution)/shard_map/all_gather | solution.py:45
  72.8 7.1 %all-to-all-start = ((bf16[2,512,1024]{1,2,0:T(8,128)(2,1)}), bf16[2,512,1024]{1,2,0:T(8,128)(2,1)S(1)}, u32[]{:S(2)}, u32[]{:S(2)}) async-start(bf16[2,512,1024]{1,2,0:T(8,128)(2,1)} %broadcast_in_dim.8), calls=%async_computation | async-start | bytes 4194304 | tf_op jit(solution)/shard_map/all_to_all | solution.py:17
  182.3 148.2 %copy-start.7 = (bf16[512,2048]{0,1:T(8,128)(2,1)S(1)}, bf16[512,2048]{0,1:T(8,128)(2,1)}, u32[]{:S(2)}) copy-start(bf16[512,2048]{0,1:T(8,128)(2,1)} %fusion.11) | copy-start | bytes 6291460
  182.3 148.2 %copy-start.36 = (f32[1024]{0:T(1024)S(1)}, f32[1024]{0:T(1024)}, u32[]{:S(2)}) copy-start(f32[1024]{0:T(1024)} %param.24) | copy-start | bytes 12292
  447.7 9.2 %copy-start.19 = (f32[2,1024]{1,0:T(2,128)S(1)}, f32[2,1024]{1,0:T(2,128)}, u32[]{:S(2)}) copy-start(f32[2,1024]{1,0:T(2,128)} %slice.293) | copy-start | bytes 24580
  447.7 9.2 %copy-start.20 = (f32[2,1024]{1,0:T(2,128)S(1)}, f32[2,1024]{1,0:T(2,128)}, u32[]{:S(2)}) copy-start(f32[2,1024]{1,0:T(2,128)} %slice.294) | copy-start | bytes 24580
  447.7 9.2 %copy-start.21 = (f32[2,1024]{1,0:T(2,128)S(1)}, f32[2,1024]{1,0:T(2,128)}, u32[]{:S(2)}) copy-start(f32[2,1024]{1,0:T(2,128)} %slice.295) | copy-start | bytes 24580
  447.7 9.2 %copy-start.22 = (f32[2,1024]{1,0:T(2,128)S(1)}, f32[2,1024]{1,0:T(2,128)}, u32[]{:S(2)}) copy-start(f32[2,1024]{1,0:T(2,128)} %slice.297) | copy-start | bytes 24580
  447.7 10.1 %copy-start.17 = (f32[3,1024]{1,0:T(4,128)S(1)}, f32[3,1024]{1,0:T(4,128)}, u32[]{:S(2)}) copy-start(f32[3,1024]{1,0:T(4,128)} %slice.286) | copy-start | bytes 36868
  447.7 10.1 %copy-start.18 = (f32[3,1024]{1,0:T(4,128)S(1)}, f32[3,1024]{1,0:T(4,128)}, u32[]{:S(2)}) copy-start(f32[3,1024]{1,0:T(4,128)} %slice.303) | copy-start | bytes 36868
  447.7 10.1 %copy-start.27 = (f32[1,1024]{1,0:T(1,128)S(1)}, f32[1,1024]{1,0:T(1,128)}, u32[]{:S(2)}) copy-start(f32[1,1024]{1,0:T(1,128)} %slice.326) | copy-start | bytes 12292
  447.7 10.2 %copy-start.15 = (f32[7,1024]{1,0:T(8,128)S(1)}, f32[7,1024]{1,0:T(8,128)}, u32[]{:S(2)}) copy-start(f32[7,1024]{1,0:T(8,128)} %slice.280) | copy-start | bytes 86020
  447.7 10.2 %copy-start.16 = (f32[7,1024]{1,0:T(8,128)S(1)}, f32[7,1024]{1,0:T(8,128)}, u32[]{:S(2)}) copy-start(f32[7,1024]{1,0:T(8,128)} %slice.305) | copy-start | bytes 86020
  447.7 10.2 %copy-start.26 = (f32[1,1024]{1,0:T(1,128)S(1)}, f32[1,1024]{1,0:T(1,128)}, u32[]{:S(2)}) copy-start(f32[1,1024]{1,0:T(1,128)} %slice.325) | copy-start | bytes 12292
  (23 other events, 62.0 us)
Sparse Core Ops, SparseCore 0:
  14.7 24.8 all-gather.10
  41.3 27.6 all-gather.16
  70.6 48.5 all-gather.12
  120.7 61.5 all-gather.18
  183.8 146.6 all-gather.8
  332.0 173.6 all-gather.14
where the time goes:
time: 569 us; the launch traced here: 565 us
  waiting for transfers between devices  287 us (50%)
  local copies, waits for them, and re-layouts  127 us (22%)
  blocking collectives  48.8 us (9%)
  other arithmetic  42.3 us (7%)
  matrix products  41.5 us (7%)
  between operations  14.2 us (2%)
    all_gather x2, waiting for transfers between devices, sent_together(): lax.all_gather(both, axis, axis=dim, tiled=True)  142 us
    all_gather x4, waiting for transfers between devices, all_blocks(): blocks = lax.all_gather(blocks, axes[k], axis=0, tiled=True)  142 us
    slice x53, local copies, waits for them, and re-layouts, recurrence(): state = lax.associative_scan(combine, (factor, drive), axis=0)[1]  87.5 us
    all_to_all x2, blocking collectives, sent_and_summed(): blocks = lax.all_to_all(split_up(array, dim, count), axis, 0, 0, tiled=True)  31.3 us
    dot_general x2, matrix products, project_back(): return jnp.dot(acts, whole, preferred_element_type=jnp.float32)  24.7 us
    pad x16, local copies, waits for them, and re-layouts, recurrence(): state = lax.associative_scan(combine, (factor, drive), axis=0)[1]  14.1 us
    mul x7, other arithmetic, combine(): return (left[0] * right[0], right[0] * left[1] + right[1])  14 us
    dot_general x2, matrix products, project_pair(): jnp.dot(normed, first_full, preferred_element_type=jnp.float32)  12.8 us
  transfers between devices with their start and end apart: 7, of which 6 were waited for; matrix products, arithmetic and copies ran while one was open for 32% of the time, Pallas kernels for 0%

commit v1 on v0

v1 whole, which is shorter than its diff:
```python
import jax
import jax.numpy as jnp
from jax import lax
from jax.experimental import pallas as pl
from jax.experimental.pallas import tpu as pltpu
from jax.sharding import Mesh
from jax.sharding import PartitionSpec as P

FS = ("fs_0", "fs_1", "fs_2")
REP_FS = ("rep", "fs_0", "fs_1", "fs_2")

EPS = 1e-06
RATE = 8.0
F32 = jnp.float32
BF16 = jnp.bfloat16
CB = 256
LANES = 128


def sigmoid(v):
    return 0.5 + 0.5 * jnp.tanh(0.5 * v)


def normed_rows(values, gain):
    scale = lax.rsqrt(jnp.mean(values * values, axis=-1, keepdims=True) + EPS)
    return (values * scale * gain).astype(BF16)


def dot(a, b):
    return jnp.dot(a, b, preferred_element_type=F32)


def dot_t(a, b):
    return lax.dot_general(a, b, (((1,), (1,)), ((), ())), preferred_element_type=F32)


def mixer_kernel(
    tok, gain, weights, in_scale, gate_scale, taps, gate_maps, rate, extra,
    partial, win, wgate, wout, xn, xpad, a_s, b_s, gel, gated, sems,
):
    length, width = tok.shape
    chans = in_scale.shape[1]
    half = width
    nblk = chans // CB
    copies = []
    for k in range(nblk):
        cols = pl.ds(k * CB, CB)
        for r, dst in ((0, win), (1, wgate)):
            copy = pltpu.make_async_copy(
                weights.at[pl.ds(r * half, half), cols], dst.at[:, cols], sems.at[r, k]
            )
            copy.start()
            copies.append(copy)
    kout = wout.shape[2]
    out_copies = []
    for r in range(2):
        copy = pltpu.make_async_copy(
            weights.at[pl.ds(r * half, half), pl.ds(chans, kout)], wout.at[r], sems.at[2, r]
        )
        copy.start()
        out_copies.append(copy)

    xn[...] = normed_rows(tok[...].astype(F32), gain[...])
    xpad[0:8, :] = jnp.zeros((8, CB), F32)
    groups = chans // LANES
    for k in range(nblk):
        cols = slice(k * CB, (k + 1) * CB)
        copies[2 * k].wait()
        pre = dot(xn[...], win[:, cols]) * in_scale[:, cols]
        xpad[8 : 8 + length, :] = pre.astype(BF16).astype(F32)
        conv = taps[3:4, cols] * xpad[8 : 8 + length, :]
        for j in range(3):
            conv = conv + taps[j : j + 1, cols] * xpad[5 + j : 5 + j + length, :]
        maps = dot(conv.astype(BF16), gate_maps[k])
        recur = sigmoid(maps[:, :CB])
        ingate = sigmoid(maps[:, CB:])
        factor = jnp.exp(rate[:, cols] * recur - extra[...])
        rest = 1.0 - factor * factor
        drive = rest * lax.rsqrt(rest) * (ingate * conv)
        for g in range(CB // LANES):
            row = k * (CB // LANES) + g
            part = slice(g * LANES, (g + 1) * LANES)
            a_s[pl.ds(row, length, stride=groups), :] = factor[:, part]
            b_s[pl.ds(row, length, stride=groups), :] = drive[:, part]
        copies[2 * k + 1].wait()
        pre_gate = (dot(xn[...], wgate[:, cols]) * gate_scale[:, cols]).astype(BF16)
        gel[:, cols] = jax.nn.gelu(pre_gate.astype(F32), approximate=True)

    step = 16

    def scan(i, h):
        base = pl.multiple_of(i * (step * groups), step * groups)
        for s in range(step):
            rows = pl.ds(base + s * groups, groups)
            h = a_s[rows, :] * h + b_s[rows, :]
            b_s[rows, :] = h
        return h

    lax.fori_loop(0, length // step, scan, jnp.zeros((groups, LANES), F32))
    for g in range(groups):
        cols = slice(g * LANES, (g + 1) * LANES)
        gated[:, cols] = (b_s[pl.ds(g, length, stride=groups), :] * gel[:, cols]).astype(BF16)
    for copy in out_copies:
        copy.wait()
    nout = 512
    for k in range(width // nout):
        rows = slice(k * nout, (k + 1) * nout)
        acc = dot_t(gated[:, :kout], wout[0, rows, :]) + dot_t(gated[:, kout:], wout[1, rows, :])
        partial[:, rows] = acc.astype(BF16)


def ffn_kernel(
    place, tok, mine, other, lru_scale, gain, weights, gate_scale, up_scale,
    own, send, mixed_own, wgate, wup, wdown, xn, hid, sems, *, col0, dcol0,
):
    length, width = tok.shape
    hidden = gate_scale.shape[1]
    kdown = wdown.shape[2]
    blocks = [(s, min(512, hidden - s)) for s in range(0, hidden, 512)]
    copies = []
    for k, (s, n) in enumerate(blocks):
        for r, dst in ((0, wgate), (1, wup)):
            copy = pltpu.make_async_copy(
                weights.at[pl.ds(r * width, width), pl.ds(col0 + s, n)],
                dst.at[:, pl.ds(s, n)],
                sems.at[r, k],
            )
            copy.start()
            copies.append(copy)
    down_copies = []
    for r in range(2):
        copy = pltpu.make_async_copy(
            weights.at[pl.ds(r * width, width), pl.ds(dcol0, kdown)], wdown.at[r], sems.at[2, r]
        )
        copy.start()
        down_copies.append(copy)
    total = mine[...].astype(F32) + other[...].astype(F32)
    mixed = (tok[...].astype(F32) + total * lru_scale[...]).astype(BF16)
    cols = width // 2
    tp = place[0]
    mixed_own[...] = jnp.where(tp == 0, mixed[:, :cols], mixed[:, cols:])
    xn[...] = normed_rows(mixed.astype(F32), gain[...])
    for k, (s, n) in enumerate(blocks):
        part = slice(s, s + n)
        copies[2 * k].wait()
        gate = dot(xn[...], wgate[:, part]) * gate_scale[:, part]
        copies[2 * k + 1].wait()
        up = dot(xn[...], wup[:, part]) * up_scale[:, part]
        hid[:, part] = (gate * sigmoid(gate) * up).astype(BF16)
    for copy in down_copies:
        copy.wait()
    skip = 2 * kdown - hidden
    for dst, which in ((send, 1 - tp), (own, tp)):
        rows = pl.ds(pl.multiple_of(which * cols, cols), cols)
        acc = dot_t(hid[:, :kdown], wdown[0, rows, :])
        acc = acc + dot_t(hid[:, kdown:], wdown[1, rows, skip:])
        dst[...] = acc.astype(BF16)


def local(
    tokens, mix_gain, lru_input, lru_gate, lru_input_scale, lru_gate_scale, conv_weight,
    recur_gate, input_gate, decay_rate, extra_decay, lru_output, lru_output_scale, ffn_gain,
    ffn_gate, ffn_up, ffn_gate_scale, ffn_up_scale, ffn_down, ffn_down_scale,
):
    length, cols = tokens.shape
    width = 2 * cols
    chans = lru_input.shape[1]
    hidden = ffn_gate.shape[1]
    rep = lax.axis_index("rep")
    tp = lax.axis_index("tp")
    swap = [(0, 1), (1, 0)]

    out_t, down_t = lru_output.T, ffn_down.T
    kout = chans // 2
    kdown = -(-hidden // (2 * LANES)) * LANES
    skip = hidden - kdown
    first = jnp.concatenate([lru_input, out_t[:, :kout], ffn_gate, down_t[:, :kdown]], axis=1)
    second = jnp.concatenate([lru_gate, out_t[:, kout:], ffn_up, down_t[:, skip:]], axis=1)
    mine = jnp.where(rep == 0, first, second).astype(BF16)
    weights = lax.all_gather(mine, REP_FS, axis=0, tiled=True)

    other = lax.ppermute(tokens, "tp", swap)
    full = jnp.where(
        tp == 0,
        jnp.concatenate([tokens, other], axis=1),
        jnp.concatenate([other, tokens], axis=1),
    )

    per = CB // recur_gate.shape[1]
    eye = jnp.eye(per, dtype=F32)

    def spread(maps):
        nb, bd, _ = maps.shape
        tiles = maps.reshape(nb // per, per, bd, 1, bd) * eye[None, :, None, :, None]
        return tiles.reshape(nb // per, CB, CB)

    gate_maps = jnp.concatenate([spread(recur_gate), spread(input_gate)], axis=2).astype(BF16)
    rate = -RATE * jax.nn.softplus(-decay_rate)

    vmem = pl.BlockSpec(memory_space=pltpu.VMEM)
    hbm = pl.BlockSpec(memory_space=pl.ANY)
    row = lambda v: v.reshape(1, -1)
    groups = chans // LANES
    partial = pl.pallas_call(
        mixer_kernel,
        out_shape=jax.ShapeDtypeStruct((length, width), BF16),
        in_specs=[vmem, vmem, hbm] + [vmem] * 6,
        out_specs=vmem,
        scratch_shapes=[
            pltpu.VMEM((width, chans), BF16),
            pltpu.VMEM((width, chans), BF16),
            pltpu.VMEM((2, width, kout), BF16),
            pltpu.VMEM((length, width), BF16),
            pltpu.VMEM((length + 8, CB), F32),
            pltpu.VMEM((length * groups, LANES), F32),
            pltpu.VMEM((length * groups, LANES), F32),
            pltpu.VMEM((length, chans), F32),
            pltpu.VMEM((length, chans), BF16),
            pltpu.SemaphoreType.DMA((3, chans // CB)),
        ],
        name="mixer",
    )(
        full, row(mix_gain), weights, row(lru_input_scale), row(lru_gate_scale), conv_weight,
        gate_maps, row(rate), extra_decay.reshape(-1, 1),
    )
    theirs = lax.ppermute(partial, "tp", swap)
    own, send, mixed = pl.pallas_call(
        lambda *refs: ffn_kernel(*refs, col0=chans + kout, dcol0=chans + kout + hidden),
        out_shape=[jax.ShapeDtypeStruct((length, cols), BF16)] * 3,
        in_specs=[pl.BlockSpec(memory_space=pltpu.SMEM)] + [vmem] * 5 + [hbm, vmem, vmem],
        out_specs=[vmem] * 3,
        scratch_shapes=[
            pltpu.VMEM((width, hidden), BF16),
            pltpu.VMEM((width, hidden), BF16),
            pltpu.VMEM((2, width, kdown), BF16),
            pltpu.VMEM((length, width), BF16),
            pltpu.VMEM((length, hidden), BF16),
            pltpu.SemaphoreType.DMA((3, 3)),
        ],
        name="ffn",
    )(
        tp.reshape(1).astype(jnp.int32), full, partial, theirs, row(lru_output_scale),
        row(ffn_gain), weights, row(ffn_gate_scale), row(ffn_up_scale),
    )
    got = lax.ppermute(send, "tp", swap)
    scale = lax.dynamic_slice_in_dim(ffn_down_scale, tp * cols, cols)
    total = own.astype(F32) + got.astype(F32)
    return (mixed.astype(F32) + total * scale).astype(BF16)


def solution(mesh):
    split = Mesh(
        mesh.devices.reshape(mesh.shape["rep"], 2, 4, 4, mesh.shape["tp"]),
        ("rep", "fs_0", "fs_1", "fs_2", "tp"),
    )
    in_specs = (
        P(REP_FS, "tp"),
        P(),
        P(FS, "tp"),
        P(FS, "tp"),
        P("tp"),
        P("tp"),
        P(None, "tp"),
        P("tp", None, None),
        P("tp", None, None),
        P("tp"),
        P(REP_FS),
        P("tp", FS),
        P(),
        P(),
        P(FS, "tp"),
        P(FS, "tp"),
        P("tp"),
        P("tp"),
        P("tp", FS),
        P(),
    )
    out_specs = P(REP_FS, "tp")
    return jax.shard_map(local, mesh=split, in_specs=in_specs, out_specs=out_specs, check_vma=False)
```

time: 569 us -> 221 us (0.39)
  waiting for transfers between devices: 287 us -> 144 us
  local copies, waits for them, and re-layouts: 127 us -> 11 us
  blocking collectives: 48.8 us -> 0 us
  matrix products: 41.5 us -> 0 us
  Pallas kernels: 0 us -> 38.3 us
  other arithmetic: 42.3 us -> 11.6 us
    all_gather x6 -> x1, waiting for transfers between devices: 284 us -> 139 us  [local(): weights = lax.all_gather(mine, REP_FS, axis=0, tiled=True)]
    slice x54 -> x2, local copies, waits for them, and re-layouts: 87.6 us -> 2.09 us  [the longest x1 1.1 us: local(): down_t[:, skip:]]
    dot_general x6 -> x0, matrix products: 41.5 us -> none  [the longest x2 24.7 us: project_back(): return jnp.dot(acts, whole, preferred_element_type=jnp.float32)]
    pallas_call x0 -> x2, Pallas kernels: none -> 38.3 us  [the longest x1 21.7 us: local(): pl.pallas_call(mixer_kernel, out_shape=jax.ShapeDtypeStruct((length, widt...]
    all_to_all x3 -> x0, blocking collectives: 36.8 us -> none  [the longest x2 31.3 us: sent_and_summed(): blocks = lax.all_to_all(split_up(array, dim, count), axis, 0, 0, tiled=True)]
    pad x16 -> x0, local copies, waits for them, and re-layouts: 14.1 us -> none  [recurrence(): state = lax.associative_scan(combine, (factor, drive), axis=0)[1]]
    mul x8 -> x1, other arithmetic: 14 us -> 0.61 us  [local(): rate = -RATE * jax.nn.softplus(-decay_rate)]
    all_gather x2 -> x0, blocking collectives: 12 us -> none  [all_blocks(): blocks = lax.all_gather(blocks, axes[k], axis=0, tiled=True)]
  transfers between devices with their start and end apart: 7 -> 4, of which waited for: 6 -> 3; matrix products, arithmetic and copies ran while one was open for 32% -> 6% of each run, Pallas kernels for 0% -> 0%
where the time goes in v1:
time: 221 us
  waiting for transfers between devices  144 us (65%)
  Pallas kernels  38.3 us (17%)
  between operations  13.5 us (6%)
  other arithmetic  11.6 us (5%)
  local copies, waits for them, and re-layouts  11 us (5%)
  starting transfers between devices  2.84 us (1%)
    all_gather x1, waiting for transfers between devices, local(): weights = lax.all_gather(mine, REP_FS, axis=0, tiled=True)  139 us
    pallas_call x1, Pallas kernels, local(): pl.pallas_call(mixer_kernel, out_shape=jax.ShapeDtypeStruct((length, widt...  21.7 us
    pallas_call x1, Pallas kernels, local(): pl.pallas_call(lambda *refs: ffn_kernel(*refs, col0=chans + kout, dcol0=c...  16.6 us
    mul x6, local copies, waits for them, and re-layouts, spread(): maps.reshape(nb // per, per, bd, 1, bd) * eye[None, :, None, :, None]  5.5 us
    select_n x1, other arithmetic, local(): jnp.where(tp == 0, jnp.concatenate([tokens, other], axis=1), jnp.concaten...  4.44 us
  transfers between devices with their start and end apart: 4, of which 3 were waited for; matrix products, arithmetic and copies ran while one was open for 6% of the time, Pallas kernels for 0%

profile of v1, /device:TPU:1, one launch (start us, length us, event | category | flops | bytes accessed | tf_op | source)
XLA Modules:
  0.0 221.1 jit_solution(11209694103380301978)
XLA Ops:
  6.5 1.1 fusion.3
  7.6 1.0 fusion.4
  8.6 2.1 fusion
  10.8 1.5 collective-permute-start
  12.2 0.4 mul.62
  12.6 1.1 mul.63
  13.8 1.4 mul.69
  15.2 2.1 mul.70
  17.4 0.3 mul.65
  17.8 0.9 copy.21.extra
  18.9 1.1 pad_maximum_fusion.gate_maps
  20.0 0.6 fusion.1
  20.6 4.4 %maximum_select_fusion.tok.refs_1_ = bf16[512,2048]{1,0:T(8,128)(2,1)} fusion(bf16[512,1024]{1,0:T(8,128)(2,1)} %collective-permute-done, bf16[512,1024]{1,0:T(8,128)(2,1)} %param.20, pred[]{:T(512)S(6)} %eq.15), kind=kLoop, calls=%fused_computation | loop fusion | flops 9437184 | bytes 4194305 | tf_op jit(solution)/shard_map/jit(_where)/select_n | solution.py:183
  25.0 138.6 %all-gather.2.cloned.1.call-done.weights.refs_6_ = bf16[4096,3712]{1,0:T(8,128)(2,1)} async-done(((bf16[64,3712]{1,0:T(8,128)(2,1)}), bf16[4096,3712]{1,0:T(8,128)(2,1)}) %all-gather.2.cloned.1.call-update) | async-done | bytes 30408720 | tf_op jit(solution)/shard_map/all_gather | solution.py:180
  163.6 21.7 %mixer.1.refs_2_ = bf16[512,2048]{1,0:T(8,128)(2,1)} custom-call(bf16[512,2048]{1,0:T(8,128)(2,1)} %maximum_select_fusion.tok.refs_1_, f32[1,2048]{1,0:T(1,128)} %bitcast.19, bf16[4096,3712]{1,0:T(8,128)(2,1)} %all-gather.2.cloned.1.call-done.weights.refs_6_, f32[1,1024]{1,0:T(1,128)} %bitcast.20, f32[1,1024]{1,0:T(1,128)} %bitcast.21, f32[4,1024]{1,0:T(4,128)} %taps.1, ...), custom_call_target="tpu_custom_call" | custom-call | tf_op jit(solution)/shard_map/mixer/pallas_call | solution.py:204
  185.4 0.9 collective-permute-start.1
  186.3 0.6 reshape.57.refs_7_
  186.9 0.6 reshape.58.refs_8_
  187.5 2.8 %collective-permute-done.1.refs_3_ = bf16[512,2048]{1,0:T(8,128)(2,1)S(1)} collective-permute-done((bf16[512,2048]{1,0:T(8,128)(2,1)}, bf16[512,2048]{1,0:T(8,128)(2,1)S(1)}, u32[]{:S(2)}, u32[]{:S(2)}) %collective-permute-start.1) | collective-permute-done | bytes 2097184 | tf_op jit(solution)/shard_map/ppermute | solution.py:226
  190.3 1.3 copy-done.1
  191.6 16.6 %ffn.1 = (bf16[512,1024]{1,0:T(8,128)(2,1)}, bf16[512,1024]{1,0:T(8,128)(2,1)}, bf16[512,1024]{1,0:T(8,128)(2,1)}) custom-call(s32[1]{0:T(128)} %bitcast.refs_0_, bf16[512,2048]{1,0:T(8,128)(2,1)} %maximum_select_fusion.tok.refs_1_, bf16[512,2048]{1,0:T(8,128)(2,1)} %mixer.1.refs_2_, bf16[512,2048]{1,0:T(8,128)(2,1)} %copy-done.1, f32[1,2048]{1,0:T(1,128)} %bitcast.17, ...), custom_call_target="tpu_custom_call" | custom-call | tf_op jit(solution)/shard_map/ffn/pallas_call | solution.py:227
  208.2 0.5 collective-permute-start.2
  208.6 2.5 %collective-permute-done.2 = bf16[512,1024]{1,0:T(8,128)(2,1)S(1)} collective-permute-done((bf16[512,1024]{1,0:T(8,128)(2,1)}, bf16[512,1024]{1,0:T(8,128)(2,1)S(1)}, u32[]{:S(2)}, u32[]{:S(2)}) %collective-permute-start.2) | collective-permute-done | bytes 1048608 | tf_op jit(solution)/shard_map/ppermute | solution.py:245
  211.1 3.2 %add_convert_fusion = bf16[512,1024]{1,0:T(8,128)(2,1)} fusion(bf16[512,1024]{1,0:T(8,128)(2,1)S(1)} %collective-permute-done.2, bf16[512,1024]{1,0:T(8,128)(2,1)} %get-tuple-element.9, bf16[512,1024]{1,0:T(8,128)(2,1)} %get-tuple-element.8, f32[1024]{0:T(1024)S(1)} %dynamic_slice.3), kind=kLoop, calls=%fused_computation.1 | loop fusion | flops 3670016 | bytes 4198400 | tf_op jit(solution)/shard_map/convert_element_type | solution.py:248
  (22 shorter events, 0.4 us)
Async XLA Ops:
  6.5 5.7 %copy-start.2 = (f32[16,64,64]{2,1,0:T(8,128)S(1)}, f32[16,64,64]{2,1,0:T(8,128)}, u32[]{:S(2)}) copy-start(f32[16,64,64]{2,1,0:T(8,128)} %param.27) | copy-start | bytes 786436
  6.5 157.1 %all-gather.2.cloned.1.call-start = ((), (), s32[]{:S(2)}) async-start(), calls=%async_computation | async-start | bytes 30883840 | tf_op jit(solution)/shard_map/all_gather | solution.py:180
  10.8 9.8 %collective-permute-start = (bf16[512,1024]{1,0:T(8,128)(2,1)}, bf16[512,1024]{1,0:T(8,128)(2,1)}, u32[]{:S(2)}, u32[]{:S(2)}) collective-permute-start(bf16[512,1024]{1,0:T(8,128)(2,1)} %param.20), channel_id=1, source_target_pairs={{0,1},{1,0},{2,3},{3,2},{4,5},{5,4},{6,7},{7,6},{8,9},{9,8},{10,11... | collective-permute-start | bytes 3145736 | tf_op jit(solution)/shard_map/ppermute | solution.py:182
  15.2 2.6 %copy-start.6 = (f32[512]{0:T(512)S(1)}, f32[512]{0:T(512)}, u32[]{:S(2)}) copy-start(f32[512]{0:T(512)} %param.30) | copy-start | bytes 6148
  17.3 1.4 copy-start
  18.7 1.3 copy-start.5
  163.6 22.7 %copy-start.3 = (f32[1408]{0:T(1024)S(1)}, f32[1408]{0:T(1024)}, u32[]{:S(2)}) copy-start(f32[1408]{0:T(1024)} %param.36) | copy-start | bytes 16900
  163.6 23.3 %copy-start.4 = (f32[1408]{0:T(1024)S(1)}, f32[1408]{0:T(1024)}, u32[]{:S(2)}) copy-start(f32[1408]{0:T(1024)} %param.37) | copy-start | bytes 16900
  185.4 4.9 %collective-permute-start.1 = (bf16[512,2048]{1,0:T(8,128)(2,1)}, bf16[512,2048]{1,0:T(8,128)(2,1)S(1)}, u32[]{:S(2)}, u32[]{:S(2)}) collective-permute-start(bf16[512,2048]{1,0:T(8,128)(2,1)} %mixer.1.refs_2_), channel_id=1, source_target_pairs={{0,1},{1,0},{2,3},{3,2},{4,5},{5,4},{6,7},{7,6},{8,9},{9,8},{10,11... | collective-permute-start | bytes 6291464 | tf_op jit(solution)/shard_map/ppermute | solution.py:226
  190.3 1.3 copy-start.1
  191.6 17.1 %copy-start.7 = (f32[2048]{0:T(1024)S(1)}, f32[2048]{0:T(1024)}, u32[]{:S(2)}) copy-start(f32[2048]{0:T(1024)} %param.39) | copy-start | bytes 24580
  208.2 3.0 %collective-permute-start.2 = (bf16[512,1024]{1,0:T(8,128)(2,1)}, bf16[512,1024]{1,0:T(8,128)(2,1)S(1)}, u32[]{:S(2)}, u32[]{:S(2)}) collective-permute-start(bf16[512,1024]{1,0:T(8,128)(2,1)} %get-tuple-element.10), channel_id=1, source_target_pairs={{0,1},{1,0},{2,3},{3,2},{4,5},{5,4},{6,7},{7,6},{8,9},{9,8},{10,11... | collective-permute-start | bytes 3145736 | tf_op jit(solution)/shard_map/ppermute | solution.py:245
Sparse Core Ops, SparseCore 0:
  10.9 152.6 all-gather.1
